TPU v7x, 32 devices: a whole 2x2x4 slice. The times are simulated.
32 devices in a mesh: ep: 4 (over y, x), tp: 8 (over z, core).
Axes of the slice: x: 2, y: 2, z: 4, core: 2. Of those that a mesh axis runs over, the one named last changes fastest.
Arguments:
- tokens: bfloat16 [512, 2048], P('ep'), may hold values from -32 to 32
- routes: int32 [512, 2], P('ep'), may hold values from 0 to 3, all different within a row; in each aligned block of 128 rows (0 to 127, 128 to 255, ...) at most 96 rows name the same one
- gates: float32 [512, 2], P('ep'), may hold values from 0.05 to 0.6
- cotangent: bfloat16 [512, 2048], P('ep'), may hold values from -6 to 6
- w_glu: bfloat16 [4, 2048, 1024], P('ep', None, 'tp'), may hold values from -0.125 to 0.125
- w_lin: bfloat16 [4, 2048, 1024], P('ep', None, 'tp'), may hold values from -0.125 to 0.125
- w_down: bfloat16 [4, 1024, 2048], P('ep', 'tp'), may hold values from -0.1875 to 0.1875
Outputs:
- d_tokens: bfloat16 [512, 2048], P('ep', 'tp')
- d_gates: float32 [512, 2], P('ep')
- glu_wgrad: float32 [4, 2048, 1024], P('ep', None, 'tp')
- lin_wgrad: float32 [4, 2048, 1024], P('ep', None, 'tp')
- down_wgrad: float32 [4, 1024, 2048], P('ep', 'tp')
- glu_norms: float32 [4, 2048], P('ep')
- lin_norms: float32 [4, 2048], P('ep')
- down_norms: float32 [4, 1024], P('ep', 'tp')
Inputs may be any that keep to these rules, and one draw needn't show every extreme that they name: `routes`: each row names 2 different experts. Among the 128 tokens of one aligned block no expert is named more than 96 times, and in every draw some expert is named exactly 96 times in some block.
All inputs are finite; a program needn't handle non-finite values.
Results may differ from a plain program's by a relative error of at most 0.024.
Values may be sent and summed in bfloat16 or wider, within the bound.
A program may use at most 64 MiB of HBM per device.

v0:
```python
import jax
import jax.numpy as jnp
from jax import lax
from jax.sharding import PartitionSpec as P

clamp_limit = 7.0
sigmoid_scale = 1.702


def slot_rank(pair_expert, all_experts):
    onehot = (pair_expert[:, None] == jnp.arange(all_experts, dtype=jnp.int32)[None, :]).astype(
        jnp.int32
    )
    return jnp.sum(jnp.cumsum(onehot, axis=0) * onehot, axis=1) - 1


def clamp_backward(glu_pre, lin_pre, back_proj, gate_col):
    glu_clip = jnp.minimum(glu_pre, clamp_limit)
    lin_clip = jnp.clip(lin_pre, -clamp_limit, clamp_limit)
    sig_val = jax.nn.sigmoid(sigmoid_scale * glu_clip)
    glu_act = glu_clip * sig_val
    hidden = glu_act * (lin_clip + 1.0)
    hid_grad = gate_col * back_proj
    act_slope = sig_val + sigmoid_scale * glu_clip * sig_val * (1.0 - sig_val)
    glu_grad = jnp.where(glu_pre < clamp_limit, hid_grad * (lin_clip + 1.0) * act_slope, 0.0)
    lin_grad = jnp.where(jnp.abs(lin_pre) < clamp_limit, hid_grad * glu_act, 0.0)
    return (hidden, glu_grad.astype(jnp.bfloat16), lin_grad.astype(jnp.bfloat16))


def pick_rows(source_rows, slot_token, local_experts, slot_total):
    padded = jnp.concatenate(
        [source_rows, jnp.zeros((1, source_rows.shape[1]), source_rows.dtype)], axis=0
    )
    return padded[slot_token].reshape(local_experts, slot_total, source_rows.shape[1])


def shards(tokens, routes, gates, cotangent, w_glu, w_lin, w_down):
    ep_count = lax.axis_size("ep")
    tp_count = lax.axis_size("tp")
    tok_rows, top_count = routes.shape
    local_experts = w_glu.shape[0]
    model_width = w_glu.shape[1]
    all_experts = local_experts * ep_count
    slot_cap = 3 * tok_rows * top_count // (2 * all_experts)
    slot_total = ep_count * slot_cap
    pair_count = tok_rows * top_count
    col_width = model_width // tp_count
    pair_expert = routes.reshape(-1)
    pair_slot = (
        pair_expert % local_experts * slot_total
        + pair_expert // local_experts * slot_cap
        + slot_rank(pair_expert, all_experts)
    )
    slot_pair = (
        jnp.full((local_experts * slot_total,), pair_count, jnp.int32)
        .at[pair_slot]
        .set(jnp.arange(pair_count, dtype=jnp.int32))
    )
    slot_token = slot_pair // top_count
    gate_send = jnp.concatenate([gates.reshape(-1), jnp.zeros((1,), jnp.float32)])[slot_pair]
    gate_rows = lax.all_to_all(
        gate_send.reshape(local_experts, slot_total), "ep", split_axis=1, concat_axis=1, tiled=True
    )
    col_start = lax.axis_index("tp") * col_width
    tok_send = pick_rows(
        lax.dynamic_slice_in_dim(tokens, col_start, col_width, 1),
        slot_token,
        local_experts,
        slot_total,
    )
    cot_send = pick_rows(
        lax.dynamic_slice_in_dim(cotangent, col_start, col_width, 1),
        slot_token,
        local_experts,
        slot_total,
    )
    tok_part, cot_part = (
        lax.all_to_all(tok_send, "ep", split_axis=1, concat_axis=1, tiled=True),
        lax.all_to_all(cot_send, "ep", split_axis=1, concat_axis=1, tiled=True),
    )
    tok_recv, cot_recv = (
        lax.all_gather(tok_part, "tp", axis=2, tiled=True),
        lax.all_gather(cot_part, "tp", axis=2, tiled=True),
    )
    glu_pre = jnp.einsum("erd,edf->erf", tok_recv, w_glu, preferred_element_type=jnp.float32)
    lin_pre = jnp.einsum("erd,edf->erf", tok_recv, w_lin, preferred_element_type=jnp.float32)
    back_proj = jnp.einsum("erd,efd->erf", cot_recv, w_down, preferred_element_type=jnp.float32)
    gate_col = gate_rows[:, :, None]
    hidden, glu_bf, lin_bf = clamp_backward(glu_pre, lin_pre, back_proj, gate_col)
    gate_part = jnp.sum(back_proj * hidden, axis=2)
    hidden_gated = (gate_col * hidden).astype(jnp.bfloat16)
    down_wgrad = jnp.einsum(
        "erf,erd->efd", hidden_gated, cot_recv, preferred_element_type=jnp.float32
    )
    glu_wgrad = jnp.einsum("erd,erf->edf", tok_recv, glu_bf, preferred_element_type=jnp.float32)
    lin_wgrad = jnp.einsum("erd,erf->edf", tok_recv, lin_bf, preferred_element_type=jnp.float32)
    input_part = jnp.dot(glu_bf[0], w_glu[0].T, preferred_element_type=jnp.float32)
    input_part = input_part + jnp.dot(lin_bf[0], w_lin[0].T, preferred_element_type=jnp.float32)
    grad_pieces = [
        lax.psum_scatter(input_part.astype(jnp.bfloat16), "tp", scatter_dimension=1, tiled=True)
    ]
    back_grads = lax.all_to_all(
        jnp.stack(grad_pieces), "ep", split_axis=1, concat_axis=1, tiled=True
    )
    gate_sums, glu_norms, lin_norms = lax.psum(
        (gate_part, jnp.sum(glu_wgrad * glu_wgrad, axis=2), jnp.sum(lin_wgrad * lin_wgrad, axis=2)),
        "tp",
    )
    gate_back = lax.all_to_all(gate_sums, "ep", split_axis=1, concat_axis=1, tiled=True)
    pair_grads = back_grads.reshape(-1, col_width)[pair_slot].astype(jnp.float32)
    d_tokens = jnp.sum(pair_grads.reshape(tok_rows, top_count, col_width), axis=1).astype(
        jnp.bfloat16
    )
    d_gates = gate_back.reshape(-1)[pair_slot].reshape(tok_rows, top_count)
    down_norms = jnp.sum(down_wgrad * down_wgrad, axis=2)
    return (d_tokens, d_gates, glu_wgrad, lin_wgrad, down_wgrad, glu_norms, lin_norms, down_norms)


def solution(mesh):
    in_specs = (
        P("ep", None),
        P("ep", None),
        P("ep", None),
        P("ep", None),
        P("ep", None, "tp"),
        P("ep", None, "tp"),
        P("ep", "tp", None),
    )
    out_specs = (
        P("ep", "tp"),
        P("ep", None),
        P("ep", None, "tp"),
        P("ep", None, "tp"),
        P("ep", "tp", None),
        P("ep", None),
        P("ep", None),
        P("ep", "tp"),
    )
    return jax.shard_map(shards, mesh=mesh, in_specs=in_specs, out_specs=out_specs, check_vma=False)
```

profile of v0, /device:TPU:0, one launch (start us, length us, event | category | flops | bytes accessed | tf_op | source)
XLA Modules:
  0.0 152.5 jit_solution(98771534761173949)
XLA Ops:
  7.2 0.7 broadcast_multiply_fusion
  8.0 0.8 copy.41
  8.9 0.1 eq.27
  9.1 0.1 mul.95
  9.3 1.2 reduce-window.6
  11.0 1.4 scatter_custom_fusion
  12.4 0.9 constant_dynamic-slice_fusion
  13.3 2.1 %gather_fusion.2 = bf16[384,256]{1,0:T(8,128)(2,1)S(1)} fusion(bf16[129,256]{1,0:T(8,128)(2,1)S(1)} %concatenate.11, s32[1024]{0:T(1024)S(1)} %get-tuple-element.58), kind=kCustom, calls=%fused_computation.2 | custom fusion | bytes 394752 | tf_op jit(solution)/shard_map/gather | solution.py:34
  15.4 0.3 copy.63
  15.7 0.5 broadcast.208
  16.2 1.8 %reduce.17 = bf16[384,256]{1,0:T(8,128)(2,1)S(1)} reduce(bf16[384,1,256]{2,1,0:T(2,128)(2,1)S(1)} %bitcast.91, bf16[]{:T(256)} %broadcast.208), dimensions={1}, to_apply=%bitcast.82.reduce_sub_computation | reduce | bytes 393218
  18.1 10.5 %all_to_all.33 = bf16[4,2,12288]{2,1,0:T(2,128)(2,1)S(1)} all-to-all(bf16[4,2,12288]{2,1,0:T(2,128)(2,1)S(1)} %reshape.251), channel_id=1, replica_groups=mesh['ep'=4,'tp'=8] {'ep'}, dimensions={0} | all-to-all | bytes 393216 | tf_op jit(solution)/shard_map/all_to_all | solution.py:79
  28.6 0.2 reshape.252
  28.8 0.7 copy.49
  29.6 2.1 %gather_fusion = bf16[384,256]{1,0:T(8,128)(2,1)S(1)} fusion(bf16[129,256]{1,0:T(8,128)(2,1)S(1)} %concatenate.9, s32[1024]{0:T(1024)S(1)} %get-tuple-element.58), kind=kCustom, calls=%fused_computation | custom fusion | bytes 394752 | tf_op jit(solution)/shard_map/gather | solution.py:34
  31.7 0.3 copy.64
  32.0 1.8 %reduce.18 = bf16[384,256]{1,0:T(8,128)(2,1)S(1)} reduce(bf16[384,1,256]{2,1,0:T(2,128)(2,1)S(1)} %bitcast.93, bf16[]{:T(256)} %broadcast.208), dimensions={1}, to_apply=%bitcast.83.reduce_sub_computation | reduce | bytes 393218
  33.8 7.9 %all_to_all.34 = bf16[4,2,12288]{2,1,0:T(2,128)(2,1)S(1)} all-to-all(bf16[4,2,12288]{2,1,0:T(2,128)(2,1)S(1)} %reshape.249), channel_id=1, replica_groups=mesh['ep'=4,'tp'=8] {'ep'}, dimensions={0} | all-to-all | bytes 393216 | tf_op jit(solution)/shard_map/all_to_all | solution.py:78
  41.8 0.2 reshape.250
  42.0 0.7 copy.46
  43.0 2.8 %gather_fusion.1 = f32[384]{0:T(512)S(1)} fusion(f32[257]{0:T(512)S(1)} %pad_maximum_fusion, s32[1024]{0:T(1024)S(1)} %get-tuple-element.57), kind=kCustom, calls=%fused_computation.1 | custom fusion | bytes 4608 | tf_op jit(solution)/shard_map/gather | solution.py:60
  45.9 7.1 %all_to_all.35 = f32[1,4,96]{2,0,1:T(1,128)S(1)} all-to-all(f32[1,4,96]{2,0,1:T(1,128)S(1)} %all_to_all.22), channel_id=1, replica_groups=mesh['ep'=4,'tp'=8] {'ep'}, dimensions={1} | all-to-all | bytes 3072 | tf_op jit(solution)/shard_map/all_to_all | solution.py:61
  53.0 0.5 broadcast.200
  53.6 0.7 reduce.15
  54.3 2.0 %all-gather.5.cloned.1.call-done = bf16[1,384,2048]{2,1,0:T(8,128)(2,1)} async-done(((bf16[1,384,256]{2,1,0:T(8,128)(2,1)}), bf16[1,384,2048]{2,1,0:T(8,128)(2,1)}) %all-gather.5.cloned.1.call-update) | async-done | bytes 1572880 | tf_op jit(solution)/shard_map/all_gather | solution.py:83
  56.3 2.0 %fusion.2 = f32[384,128]{0,1:T(8,128)S(1)} fusion(bf16[1,384,2048]{2,1,0:T(8,128)(2,1)} %all-gather.5.cloned.1.call-done, bf16[1,128,2048]{2,1,0:T(8,128)(2,1)S(1)} %copy-done.5), kind=kOutput, calls=%fused_computation.9 | convolution fusion | flops 201326592 | bytes 2293760 | tf_op jit(solution)/shard_map/erd,efd->erf/dot_general | solution.py:87
  58.3 26.1 %all-gather.3.cloned.1.call-done = bf16[1,384,2048]{2,1,0:T(8,128)(2,1)} async-done(((bf16[1,384,256]{2,1,0:T(8,128)(2,1)}), bf16[1,384,2048]{2,1,0:T(8,128)(2,1)}) %all-gather.3.cloned.1.call-update) | async-done | bytes 1572880 | tf_op jit(solution)/shard_map/all_gather | solution.py:82
  84.4 2.1 %fusion.10 = f32[384,128]{0,1:T(8,128)S(1)} fusion(bf16[1,384,2048]{2,1,0:T(8,128)(2,1)} %all-gather.3.cloned.1.call-done, bf16[1,2048,128]{2,1,0:T(8,128)(2,1)S(1)} %copy-done.3), kind=kOutput, calls=%fused_computation.17 | convolution fusion | flops 201326592 | bytes 2293760 | tf_op jit(solution)/shard_map/erd,edf->erf/dot_general | solution.py:85
  86.6 1.3 select_convert_fusion
  87.9 0.6 fusion.15
  88.5 1.8 %add_convert_fusion = bf16[384,2048]{1,0:T(8,128)(2,1)} fusion(f32[384,2048]{1,0:T(8,128)S(1)} %fusion.15, bf16[384,128]{0,1:T(8,128)(2,1)S(1)} %get-tuple-element.43, bf16[1,2048,128]{2,1,0:T(8,128)(2,1)S(1)} %copy-done), kind=kOutput, calls=%fused_computation.6 | convolution fusion | flops 202899456 | bytes 5341184 | tf_op jit(solution)/shard_map/dot_general | solution.py:98
  90.3 0.4 multiply_reduce_fusion.1
  90.8 1.4 multiply_reduce_fusion.2
  92.2 28.1 %all-reduce.2 = (f32[1,4,96]{2,0,1:T(1,128)}, f32[1,2048]{1,0:T(1,128)}, f32[1,2048]{1,0:T(1,128)}) all-reduce(f32[1,4,96]{2,0,1:T(1,128)S(1)} %all_to_all.26, f32[1,2048]{1,0:T(1,128)S(1)} %bitcast.99, f32[1,2048]{1,0:T(1,128)S(1)} %bitcast.98), channel_id=1, replica_groups=mesh['ep'=4,'tp'=8] {'tp'}, use_global_device_ids=true, to_apply=%region_7.8 | all-reduce | flops 4480 | bytes 35840 | tf_op jit(solution)/shard_map/psum | solution.py:105
  120.3 3.4 %all-to-all-start.4 = ((f32[1,4,96]{2,0,1:T(1,128)}), f32[1,4,96]{2,0,1:T(1,128)S(1)}, u32[]{:S(2)}, u32[]{:S(2)}) async-start(f32[1,4,96]{2,0,1:T(1,128)} %get-tuple-element.40), calls=%async_computation.5 | async-start | bytes 4096 | tf_op jit(solution)/shard_map/all_to_all | solution.py:109
  123.7 1.2 copy.62
  125.0 2.5 %reduce.19 = bf16[384,256]{1,0:T(8,128)(2,1)} reduce(bf16[384,1,256]{2,1,0:T(2,128)(2,1)S(1)} %bitcast.92, bf16[]{:T(256)} %broadcast.208), dimensions={1}, to_apply=%bitcast.81.reduce_sub_computation | reduce | bytes 393218
  127.4 1.6 %reshape.253 = bf16[4,2,12288]{2,1,0:T(2,128)(2,1)} reshape(bf16[384,256]{1,0:T(8,128)(2,1)} %reduce.19) | data formatting | bytes 393216
  129.1 4.2 %all-to-all-start.3 = ((bf16[4,2,12288]{2,1,0:T(2,128)(2,1)}), bf16[4,2,12288]{2,1,0:T(2,128)(2,1)S(1)}, u32[]{:S(2)}, u32[]{:S(2)}) async-start(bf16[4,2,12288]{2,1,0:T(2,128)(2,1)} %reshape.253), calls=%async_computation.4 | async-start | bytes 393216 | tf_op jit(solution)/shard_map/all_to_all | solution.py:102
  133.3 3.0 %multiply_reduce_fusion = (f32[128]{0:T(128)}, f32[128,2048]{1,0:T(8,128)}) fusion(bf16[1,384,2048]{2,1,0:T(8,128)(2,1)S(1)} %copy-done.2, f32[384]{0:T(512)S(1)} %mul.97, f32[384,128]{0,1:T(8,128)} %get-tuple-element.48, f32[384,128]{0,1:T(8,128)} %copy-done.4), kind=kOutput, calls=%fused_computation.19 | convolution fusion | flops 202391424 | bytes 3016704 | tf_op jit(solution)/shard_map/erf,erd->efd/dot_general | solution.py:92
  136.2 2.5 %copy.52 = f32[1,2048,128]{2,1,0:T(8,128)} copy(f32[1,2048,128]{1,2,0:T(8,128)} %bitcast.87) | data formatting | bytes 2097152
  138.8 1.3 copy.53
  140.1 0.7 reduce.16
  140.8 1.9 %gather_fusion.4 = f32[256]{0:T(256)S(1)} fusion(f32[384]{0:T(512)S(1)} %reshape.177, s32[1024]{0:T(1024)S(1)} %pad_clamp_fusion), kind=kCustom, calls=%fused_computation.4 | custom fusion | bytes 3072 | tf_op jit(solution)/shard_map/gather | solution.py:114
  142.9 0.6 copy.51
  143.6 0.2 reshape.254
  143.8 1.2 gather_fusion.3
  145.0 1.0 reduce_sum.66
  (53 shorter events, 1.9 us)
Async XLA Ops:
  7.2 79.4 %copy-start = (bf16[1,2048,128]{2,1,0:T(8,128)(2,1)S(1)}, bf16[1,2048,128]{2,1,0:T(8,128)(2,1)}, u32[]{:S(2)}) copy-start(bf16[1,2048,128]{2,1,0:T(8,128)(2,1)} %param.12) | copy-start | bytes 1572868
  7.2 49.1 %all-gather.5.cloned.1.call-start = ((), (), s32[]{:S(2)}) async-start(), calls=%async_computation.7 | async-start | bytes 1769472 | tf_op jit(solution)/shard_map/all_gather | solution.py:83
  29.5 54.9 %all-gather.3.cloned.1.call-start = ((), (), s32[]{:S(2)}) async-start(), calls=%async_computation.6 | async-start | bytes 1769472 | tf_op jit(solution)/shard_map/all_gather | solution.py:82
  31.6 11.1 %copy-start.6 = (f32[128,2]{0,1:T(2,128)S(1)}, f32[128,2]{0,1:T(2,128)}, u32[]{:S(2)}) copy-start(f32[128,2]{0,1:T(2,128)} %param.9) | copy-start | bytes 3076
  41.9 14.4 %copy-start.5 = (bf16[1,128,2048]{2,1,0:T(8,128)(2,1)S(1)}, bf16[1,128,2048]{2,1,0:T(8,128)(2,1)}, u32[]{:S(2)}) copy-start(bf16[1,128,2048]{2,1,0:T(8,128)(2,1)} %param.13) | copy-start | bytes 1572868
  42.7 81.0 %reduce-scatter.2.cloned.1.call-start = ((), (), s32[]{:S(2)}) async-start(), calls=%async_computation.8 | async-start | bytes 1769472 | tf_op jit(solution)/shard_map/reduce_scatter | solution.py:100
  45.8 38.6 %copy-start.3 = (bf16[1,2048,128]{2,1,0:T(8,128)(2,1)S(1)}, bf16[1,2048,128]{2,1,0:T(8,128)(2,1)}, u32[]{:S(2)}) copy-start(bf16[1,2048,128]{2,1,0:T(8,128)(2,1)} %param.11) | copy-start | bytes 1572868
  84.4 2.1 %copy-start.1 = (bf16[1,384,2048]{2,1,0:T(8,128)(2,1)S(1)}, bf16[1,384,2048]{2,1,0:T(8,128)(2,1)}, u32[]{:S(2)}) copy-start(bf16[1,384,2048]{2,1,0:T(8,128)(2,1)} %all-gather.3.cloned.1.call-done) | copy-start | bytes 4718596
  86.5 1.3 copy-start.4
  92.2 41.1 %copy-start.2 = (bf16[1,384,2048]{2,1,0:T(8,128)(2,1)S(1)}, bf16[1,384,2048]{2,1,0:T(8,128)(2,1)}, u32[]{:S(2)}) copy-start(bf16[1,384,2048]{2,1,0:T(8,128)(2,1)} %all-gather.5.cloned.1.call-done) | copy-start | bytes 4718596
  120.3 8.8 %all-to-all-start.4 = ((f32[1,4,96]{2,0,1:T(1,128)}), f32[1,4,96]{2,0,1:T(1,128)S(1)}, u32[]{:S(2)}, u32[]{:S(2)}) async-start(f32[1,4,96]{2,0,1:T(1,128)} %get-tuple-element.40), calls=%async_computation.5 | async-start | bytes 4096 | tf_op jit(solution)/shard_map/all_to_all | solution.py:109
  129.1 14.5 %all-to-all-start.3 = ((bf16[4,2,12288]{2,1,0:T(2,128)(2,1)}), bf16[4,2,12288]{2,1,0:T(2,128)(2,1)S(1)}, u32[]{:S(2)}, u32[]{:S(2)}) async-start(bf16[4,2,12288]{2,1,0:T(2,128)(2,1)} %reshape.253), calls=%async_computation.4 | async-start | bytes 393216 | tf_op jit(solution)/shard_map/all_to_all | solution.py:102
Sparse Core Ops, SparseCore 0:
  29.6 26.6 all-gather.4
  58.5 25.8 all-gather.2
  90.4 33.0 reduce-scatter.1
where the time goes:
time: 153 us; the launch traced here: 152 us
  blocking collectives  53.7 us (35%)
  waiting for transfers between devices  28.2 us (18%)
  local copies, waits for them, and re-layouts  25.8 us (17%)
  between operations  14.1 us (9%)
  matrix products  12.6 us (8%)
  other arithmetic  10.5 us (7%)
  starting transfers between devices  7.7 us (5%)
    psum x1, blocking collectives, shards(): lax.psum((gate_part, jnp.sum(glu_wgrad * glu_wgrad, axis=2), jnp.sum(lin_...  28.1 us
    all_gather x1, waiting for transfers between devices, shards(): lax.all_gather(tok_part, 'tp', axis=2, tiled=True)  26.1 us
    all_to_all x1, blocking collectives, shards(): lax.all_to_all(cot_send, 'ep', split_axis=1, concat_axis=1, tiled=True)  10.5 us
    unnamed x27, local copies, waits for them, and re-layouts  8.22 us
    all_to_all x1, blocking collectives, shards(): lax.all_to_all(tok_send, 'ep', split_axis=1, concat_axis=1, tiled=True)  7.92 us
    all_to_all x1, blocking collectives, shards(): lax.all_to_all(gate_send.reshape(local_experts, slot_total), 'ep', split_...  7.13 us
    unnamed x4, other arithmetic  6.17 us
    all_to_all x1, starting transfers between devices, shards(): lax.all_to_all(jnp.stack(grad_pieces), 'ep', split_axis=1, concat_axis=1,...  4.17 us
  transfers between devices with their start and end apart: 5, of which 2 were waited for; matrix products, arithmetic and copies ran while one was open for 19% of the time, Pallas kernels for 0%

commit v1 on v0

v1 whole, which is shorter than its diff:
```python
import functools

import jax
import jax.numpy as jnp
from jax import lax
from jax.experimental import pallas as pl
from jax.experimental.pallas import tpu as pltpu
from jax.sharding import PartitionSpec as P

clamp_limit = 7.0
sigmoid_scale = 1.702
MESH = pl.DeviceIdType.MESH
LANES = 128
CORES = 2
f32 = jnp.float32
bf16 = jnp.bfloat16


def dot_nn(a, b):
    return lax.dot_general(a, b, (((1,), (0,)), ((), ())), preferred_element_type=f32)


def dot_nt(a, b):
    return lax.dot_general(a, b, (((1,), (1,)), ((), ())), preferred_element_type=f32)


def clamp_backward(glu_pre, lin_pre, back_proj, gate_col):
    glu_clip = jnp.minimum(glu_pre, clamp_limit)
    lin_clip = jnp.clip(lin_pre, -clamp_limit, clamp_limit)
    sig_val = jax.nn.sigmoid(sigmoid_scale * glu_clip)
    glu_act = glu_clip * sig_val
    hidden = glu_act * (lin_clip + 1.0)
    hid_grad = gate_col * back_proj
    act_slope = sig_val + sigmoid_scale * glu_clip * sig_val * (1.0 - sig_val)
    glu_grad = jnp.where(glu_pre < clamp_limit, hid_grad * (lin_clip + 1.0) * act_slope, 0.0)
    lin_grad = jnp.where(jnp.abs(lin_pre) < clamp_limit, hid_grad * glu_act, 0.0)
    return hidden, glu_grad.astype(bf16), lin_grad.astype(bf16)


def kernel(
    ep, tp, cap,
    tok_ref, routes_ref, gates_ref, cot_ref, wg_ref, wl_ref, wd_ref,
    dtok_ref, dgate_ref, gw_ref, lw_ref, dw_ref, gn_ref, ln_ref, dn_ref,
    pt_v, snd_v, all_v, gsnd_v, grow_v, bf_v, tr_v,
    ps_v, pr_v, mine_v, xs_v, ret_v, zs_v, zr_v,
    gp_v, gsum_v, gback_v, ns_v, nr_v, gw_v, lw_v, dw_v,
    d_s, d_r, g_s, g_r, y_s, y_r, p_s, p_r, x_s, x_r, z_s, z_r,
    a_s, a_r, b_s, b_r, n_s, n_r, o_s,
):
    me = lax.axis_index("ep")
    tpi = lax.axis_index("tp")
    nz = tp // CORES
    core = lax.rem(tpi, CORES)
    chip = lax.div(tpi, CORES)
    other = 1 - core
    partner = chip * CORES + other
    rows = tok_ref.shape[0]
    width = tok_ref.shape[1]
    hidden_units = wg_ref.shape[1]
    half = width // CORES
    own = width // tp

    def ahead(r):
        return lax.rem(me + r, ep)

    def behind(r):
        return lax.rem(me + ep - r, ep)

    barrier = pltpu.get_barrier_semaphore()
    for r in range(1, ep):
        pl.semaphore_signal(barrier, inc=1, device_id={"ep": ahead(r)}, device_id_type=MESH)
    for q in range(1, tp):
        pl.semaphore_signal(
            barrier, inc=1, device_id={"tp": lax.rem(tpi + q, tp)}, device_id_type=MESH
        )

    def remote(src, dst, ss, rs, where):
        return pltpu.make_async_remote_copy(
            src_ref=src, dst_ref=dst, send_sem=ss, recv_sem=rs,
            device_id=where, device_id_type=MESH,
        )

    rel = routes_ref[...] - me
    rel = jnp.where(rel < 0, rel + ep, rel)
    lane = lax.broadcasted_iota(jnp.int32, (rows, LANES), 1)
    first, second = lane == rel[:, 0:1], lane == rel[:, 1:2]
    mask = jnp.where(first, 1.0, 0.0) + jnp.where(second, 1.0, 0.0)
    gate_of = jnp.where(first, gates_ref[:, 0:1], 0.0) + jnp.where(second, gates_ref[:, 1:2], 0.0)
    before = lax.broadcasted_iota(jnp.int32, (rows, rows), 1) < lax.broadcasted_iota(
        jnp.int32, (rows, rows), 0
    )
    rank = dot_nn(jnp.where(before, 1.0, 0.0).astype(bf16), mask.astype(bf16))
    place = jnp.where(mask > 0.5, rank, -1.0)
    lane_f = lane.astype(f32)
    sends = []
    picks = []
    for r in range(ep):
        hit = jnp.where(lane_f == place[:, r:r + 1], 1.0, 0.0)
        pt_v[r] = hit.astype(bf16)
        picks.append(hit.T[:cap, :].astype(bf16))
        row = jnp.sum(hit * gate_of[:, r:r + 1], axis=0, keepdims=True)
        if r == 0:
            grow_v[0] = jnp.broadcast_to(row, (8, LANES))
        else:
            gsnd_v[r] = jnp.broadcast_to(row, (8, LANES))
    half_cols = pl.ds(pl.multiple_of(core * half, half), half)
    waited = False
    for r in range(1, ep):
        for a, ref in ((0, tok_ref), (1, cot_ref)):
            snd_v[a, r] = dot_nn(picks[r], ref[:, half_cols]).astype(bf16)
            if not waited:
                pl.semaphore_wait(barrier, ep - 1 + tp - 1)
                waited = True
            cp = remote(
                snd_v.at[a, r], all_v.at[a, core, pl.ds(r * cap, cap), :],
                d_s.at[a, r], d_r.at[a, r], {"ep": ahead(r)},
            )
            cp.start()
            sends.append(cp)
        cp = remote(gsnd_v.at[r], grow_v.at[r], g_s.at[r], g_r.at[r], {"ep": ahead(r)})
        cp.start()
        sends.append(cp)
    for a, ref in ((0, tok_ref), (1, cot_ref)):
        for h in range(CORES):
            all_v[a, h, 0:cap, :] = dot_nn(picks[0], ref[:, h * half:(h + 1) * half]).astype(bf16)

    eye = lax.broadcasted_iota(jnp.int32, (cap, LANES), 0) == lax.broadcasted_iota(
        jnp.int32, (cap, LANES), 1
    )

    gp_v[tpi] = jnp.zeros(gp_v.shape[1:], f32)

    def forward(r):
        rs = slice(r * cap, (r + 1) * cap)
        glu_pre = jnp.zeros((cap, hidden_units), f32)
        lin_pre = glu_pre
        back = glu_pre
        for h in range(CORES):
            hs = slice(h * half, (h + 1) * half)
            glu_pre = glu_pre + dot_nn(all_v[0, h, rs, :], wg_ref[hs, :])
            lin_pre = lin_pre + dot_nn(all_v[0, h, rs, :], wl_ref[hs, :])
            back = back + dot_nt(all_v[1, h, rs, :], wd_ref[:, hs])
        gate_col = jnp.sum(jnp.where(eye, grow_v[r, 0:1, :], 0.0), axis=1, keepdims=True)
        hidden, glu_bf, lin_bf = clamp_backward(glu_pre, lin_pre, back, gate_col)
        part = jnp.sum(back * hidden, axis=1, keepdims=True)
        gp_v[tpi, r:r + 1, :] = jnp.sum(jnp.where(eye, part, 0.0), axis=0, keepdims=True)
        bf_v[0, rs, :] = glu_bf
        bf_v[1, rs, :] = lin_bf
        bf_v[2, rs, :] = (gate_col * hidden).astype(bf16)

    forward(0)
    relays = []
    for r in range(1, ep):
        for a in range(2):
            mine = all_v.at[a, core, pl.ds(r * cap, cap), :]
            remote(snd_v.at[a, r], mine, d_s.at[a, r], d_r.at[a, r], {"ep": ahead(r)}).wait_recv()
            cp = remote(mine, mine, y_s.at[a, r], y_r.at[a, r], {"tp": partner})
            cp.start()
            relays.append(cp)
    for r in range(1, ep):
        for a in range(2):
            theirs = all_v.at[a, other, pl.ds(r * cap, cap), :]
            remote(theirs, theirs, y_s.at[a, r], y_r.at[a, r], {"tp": partner}).wait_recv()
        remote(gsnd_v.at[r], grow_v.at[r], g_s.at[r], g_r.at[r], {"ep": ahead(r)}).wait_recv()
        forward(r)

    for q in range(1, tp):
        cp = remote(gp_v.at[tpi], gp_v.at[tpi], a_s.at[q], a_r.at[q], {"tp": lax.rem(tpi + q, tp)})
        cp.start()
        sends.append(cp)

    def input_cols(q, which):
        z = lax.rem(chip + q, nz)
        at = pl.ds(pl.multiple_of((z * CORES + which) * own, own), own)
        return dot_nt(bf_v[0], wg_ref[at, :]) + dot_nt(bf_v[1], wl_ref[at, :])

    order = list(range(1, nz)) + [0]
    for q in order:
        ps_v[q] = input_cols(q, other).astype(bf16)
        cp = remote(ps_v.at[q], pr_v.at[q], p_s.at[q], p_r.at[q], {"tp": partner})
        cp.start()
        sends.append(cp)
    for q in order:
        mine_v[q] = input_cols(q, core)
    for q in order:
        remote(ps_v.at[q], pr_v.at[q], p_s.at[q], p_r.at[q], {"tp": partner}).wait_recv()
        total = (mine_v[q] + pr_v[q].astype(f32)).astype(bf16)
        ret_v[q, 0:cap, :] = total[0:cap, :]
        for r in range(1, ep):
            rs = slice(r * cap, (r + 1) * cap)
            xs_v[q, rs, :] = total[rs, :]
        for r in range(1, ep):
            rs = pl.ds(r * cap, cap)
            cp = remote(
                xs_v.at[q, rs, :], ret_v.at[q, rs, :],
                x_s.at[q, r], x_r.at[q, r], {"ep": behind(r)},
            )
            cp.start()
            sends.append(cp)

    for i in range(3):
        tr_v[i] = bf_v[i].astype(f32).T.astype(bf16)
    step = min(512, half)
    outs = []
    for h in range(CORES):
        for c0 in range(0, half, step):
            cols = slice(h * half + c0, h * half + c0 + step)
            x = all_v[0, h, :, c0:c0 + step]
            for i, (w_v, at) in enumerate(((gw_v, 0), (lw_v, 1))):
                w = dot_nn(tr_v[i], x)
                ns_v[at:at + 1, cols] = jnp.sum(w * w, axis=0, keepdims=True)
                w_v[cols, :] = w.T
    nr_v[tpi] = ns_v[...]
    for q in range(1, tp):
        cp = remote(ns_v, nr_v.at[tpi], n_s.at[q], n_r.at[q], {"tp": lax.rem(tpi + q, tp)})
        cp.start()
        sends.append(cp)
    for i, (src, dst) in enumerate(((gw_v, gw_ref), (lw_v, lw_ref))):
        cp = pltpu.make_async_copy(src, dst, o_s.at[i])
        cp.start()
        outs.append(cp)

    for q in range(1, tp):
        frm = lax.rem(tpi + tp - q, tp)
        remote(gp_v.at[tpi], gp_v.at[frm], a_s.at[q], a_r.at[q], {"tp": partner}).wait_recv()
    gsum = gp_v[0]
    for j in range(1, tp):
        gsum = gsum + gp_v[j]
    gback_v[0, 0:1, :] = gsum[0:1, :]
    for r in range(1, ep):
        gsum_v[r] = jnp.broadcast_to(gsum[r:r + 1, :], (8, LANES))
        cp = remote(gsum_v.at[r], gback_v.at[r], b_s.at[r], b_r.at[r], {"ep": behind(r)})
        cp.start()
        sends.append(cp)

    norm = jnp.zeros((hidden_units, 1), f32)
    for h in range(CORES):
        for c0 in range(0, half, step):
            cols = slice(h * half + c0, h * half + c0 + step)
            w = dot_nn(tr_v[2], all_v[1, h, :, c0:c0 + step])
            norm = norm + jnp.sum(w * w, axis=1, keepdims=True)
            dw_v[:, cols] = w
    cp = pltpu.make_async_copy(dw_v, dw_ref, o_s.at[2])
    cp.start()
    outs.append(cp)
    diag = lax.broadcasted_iota(jnp.int32, (hidden_units, hidden_units), 0) == (
        lax.broadcasted_iota(jnp.int32, (hidden_units, hidden_units), 1)
    )
    dn_ref[...] = jnp.sum(jnp.where(diag, norm, 0.0), axis=0, keepdims=True)

    acc = None
    for q in order:
        part = None
        for r in range(ep):
            rs = pl.ds(r * cap, cap)
            if r > 0:
                remote(
                    xs_v.at[q, rs, :], ret_v.at[q, rs, :],
                    x_s.at[q, r], x_r.at[q, r], {"ep": behind(r)},
                ).wait_recv()
            term = dot_nn(pt_v[r][:, :cap], ret_v[q, r * cap:(r + 1) * cap, :])
            part = term if part is None else part + term
        if q == 0:
            acc = part
        else:
            zs_v[q] = part.astype(bf16)
            to = lax.rem(chip + q, nz) * CORES + core
            cp = remote(zs_v.at[q], zr_v.at[q], z_s.at[q], z_r.at[q], {"tp": to})
            cp.start()
            sends.append(cp)

    res = [jnp.zeros((rows, 1), f32), jnp.zeros((rows, 1), f32)]
    for r in range(ep):
        if r > 0:
            remote(
                gsum_v.at[r], gback_v.at[r], b_s.at[r], b_r.at[r], {"ep": behind(r)}
            ).wait_recv()
        val = jnp.sum(pt_v[r].astype(f32) * gback_v[r, 0:1, :], axis=1, keepdims=True)
        for k in range(2):
            res[k] = res[k] + jnp.where(rel[:, k:k + 1] == r, val, 0.0)
    dgate_ref[:, 0:1] = res[0]
    dgate_ref[:, 1:2] = res[1]

    for q in range(1, tp):
        frm = lax.rem(tpi + tp - q, tp)
        remote(ns_v, nr_v.at[frm], n_s.at[q], n_r.at[q], {"tp": partner}).wait_recv()
    norms = nr_v[0]
    for j in range(1, tp):
        norms = norms + nr_v[j]
    gn_ref[...] = norms[0:1, :]
    ln_ref[...] = norms[1:2, :]

    for q in range(1, nz):
        remote(zs_v.at[q], zr_v.at[q], z_s.at[q], z_r.at[q], {"tp": partner}).wait_recv()
        acc = acc + zr_v[q].astype(f32)
    dtok_ref[...] = acc.astype(bf16)

    for cp in sends + relays:
        cp.wait_send()
    for cp in outs:
        cp.wait()


def shards(tokens, routes, gates, cotangent, w_glu, w_lin, w_down):
    ep = lax.axis_size("ep")
    tp = lax.axis_size("tp")
    rows, top = routes.shape
    width = tokens.shape[1]
    units = w_glu.shape[2]
    cap = 3 * rows * top // (2 * ep)
    cap = -(-cap // 16) * 16
    slots = ep * cap
    half = width // CORES
    own = width // tp
    nz = tp // CORES
    vm = pl.BlockSpec(memory_space=pltpu.VMEM)
    hbm = pl.BlockSpec(memory_space=pl.ANY)
    dma = pltpu.SemaphoreType.DMA
    erows = max(8, ep)
    V = pltpu.VMEM
    outs = pl.pallas_call(
        functools.partial(kernel, ep, tp, cap),
        out_shape=(
            jax.ShapeDtypeStruct((rows, own), bf16),
            jax.ShapeDtypeStruct((rows, top), f32),
            jax.ShapeDtypeStruct((width, units), f32),
            jax.ShapeDtypeStruct((width, units), f32),
            jax.ShapeDtypeStruct((units, width), f32),
            jax.ShapeDtypeStruct((1, width), f32),
            jax.ShapeDtypeStruct((1, width), f32),
            jax.ShapeDtypeStruct((1, units), f32),
        ),
        in_specs=[vm] * 7,
        out_specs=(vm, vm, hbm, hbm, hbm, vm, vm, vm),
        scratch_shapes=[
            V((ep, rows, LANES), bf16),
            V((2, ep, cap, half), bf16),
            V((2, CORES, slots, half), bf16),
            V((ep, 8, LANES), f32),
            V((ep, 8, LANES), f32),
            V((3, slots, units), bf16),
            V((3, units, slots), bf16),
            V((nz, slots, own), bf16),
            V((nz, slots, own), bf16),
            V((nz, slots, own), f32),
            V((nz, slots, own), bf16),
            V((nz, slots, own), bf16),
            V((nz, rows, own), bf16),
            V((nz, rows, own), bf16),
            V((tp, erows, LANES), f32),
            V((ep, 8, LANES), f32),
            V((ep, 8, LANES), f32),
            V((2, width), f32),
            V((tp, 2, width), f32),
            V((width, units), f32),
            V((width, units), f32),
            V((units, width), f32),
            dma((2, ep)), dma((2, ep)), dma((ep,)), dma((ep,)), dma((2, ep)), dma((2, ep)),
            dma((nz,)), dma((nz,)), dma((nz, ep)), dma((nz, ep)), dma((nz,)), dma((nz,)),
            dma((tp,)), dma((tp,)), dma((ep,)), dma((ep,)), dma((tp,)), dma((tp,)), dma((3,)),
        ],
        compiler_params=pltpu.CompilerParams(
            collective_id=0, has_side_effects=True, vmem_limit_bytes=40 * 1024 * 1024
        ),
    )(tokens, routes, gates, cotangent, w_glu[0], w_lin[0], w_down[0])
    d_tokens, d_gates, gw, lw, dw, gn, ln, dn = outs
    return (d_tokens, d_gates, gw[None], lw[None], dw[None], gn, ln, dn)


def solution(mesh):
    in_specs = (
        P("ep", None),
        P("ep", None),
        P("ep", None),
        P("ep", None),
        P("ep", None, "tp"),
        P("ep", None, "tp"),
        P("ep", "tp", None),
    )
    out_specs = (
        P("ep", "tp"),
        P("ep", None),
        P("ep", None, "tp"),
        P("ep", None, "tp"),
        P("ep", "tp", None),
        P("ep", None),
        P("ep", None),
        P("ep", "tp"),
    )
    return jax.shard_map(shards, mesh=mesh, in_specs=in_specs, out_specs=out_specs, check_vma=False)
```

time: 153 us -> 56.8 us (0.37)
  blocking collectives: 53.7 us -> 0 us
  Pallas kernels: 0 us -> 43.2 us
  waiting for transfers between devices: 28.2 us -> 0 us
  between operations: 14.1 us -> 0.66 us
  local copies, waits for them, and re-layouts: 25.8 us -> 12.5 us
  matrix products: 12.6 us -> 0 us
  other arithmetic: 10.5 us -> 0 us
  starting transfers between devices: 7.7 us -> 0 us
    pallas_call x0 -> x1, Pallas kernels: none -> 43.2 us  [shards(): pl.pallas_call(functools.partial(kernel, ep, tp, cap), out_shape=(jax.Sha...]
    all_gather x2 -> x0, waiting for transfers between devices: 28.1 us -> none  [the longest x1 26.1 us: shards(): lax.all_gather(tok_part, 'tp', axis=2, tiled=True)]
    psum x1 -> x0, blocking collectives: 28.1 us -> none  [shards(): lax.psum((gate_part, jnp.sum(glu_wgrad * glu_wgrad, axis=2), jnp.sum(lin_...]
    all_to_all x3 -> x0, blocking collectives: 25.6 us -> none  [the longest x1 10.5 us: shards(): lax.all_to_all(cot_send, 'ep', split_axis=1, concat_axis=1, tiled=True)]
    dot_general x8 -> x0, matrix products: 12.6 us -> none  [the longest x1 2.96 us: shards(): jnp.einsum('erf,erd->efd', hidden_gated, cot_recv, preferred_element_type...]
    gather x6 -> x0, local copies, waits for them, and re-layouts: 10.1 us -> none  [the longest x2 4.11 us: pick_rows(): padded[slot_token].reshape(local_experts, slot_total, source_rows.shape[1])]
    all_to_all x2 -> x0, starting transfers between devices: 7.58 us -> none  [the longest x1 4.17 us: shards(): lax.all_to_all(jnp.stack(grad_pieces), 'ep', split_axis=1, concat_axis=1,...]
    unnamed x4 -> x0, other arithmetic: 6.17 us -> none
  transfers between devices with their start and end apart: 5 -> 0, of which waited for: 2 -> 0; matrix products, arithmetic and copies ran while one was open for 19% -> 0% of each run, Pallas kernels for 0% -> 0%
where the time goes in v1:
time: 56.8 us; the launch traced here: 56.4 us
  Pallas kernels  43.2 us (76%)
  local copies, waits for them, and re-layouts  12.5 us (22%)
  between operations  0.66 us (1%)
    pallas_call x1, Pallas kernels, shards(): pl.pallas_call(functools.partial(kernel, ep, tp, cap), out_shape=(jax.Sha...  43.2 us
    unnamed x24, local copies, waits for them, and re-layouts  12.5 us

profile of v1, /device:TPU:0, one launch (start us, length us, event | category | flops | bytes accessed | tf_op | source)
XLA Modules:
  0.0 56.4 jit_solution(11974938978585908445)
XLA Ops:
  0.6 0.0 copy-start.5
  0.6 0.7 %copy-done.5 = s32[128,2]{0,1:T(2,128)S(1)} copy-done((s32[128,2]{0,1:T(2,128)S(1)}, s32[128,2]{0,1:T(2,128)}, u32[]{:S(2)}) %copy-start.5) | copy-done | bytes 1048
  1.3 0.0 copy-start.6
  1.3 0.1 copy.15.routes_ref
  1.4 0.6 %copy-done.6 = f32[128,2]{0,1:T(2,128)S(1)} copy-done((f32[128,2]{0,1:T(2,128)S(1)}, f32[128,2]{0,1:T(2,128)}, u32[]{:S(2)}) %copy-start.6) | copy-done | bytes 1048
  2.0 0.1 copy.16.gates_ref
  2.1 0.0 copy-start
  2.1 1.0 %copy-done = bf16[128,2048]{1,0:T(8,128)(2,1)S(1)} copy-done((bf16[128,2048]{1,0:T(8,128)(2,1)S(1)}, bf16[128,2048]{1,0:T(8,128)(2,1)}, u32[]{:S(2)}) %copy-start) | copy-done | bytes 524312
  3.1 0.0 copy-start.1
  3.1 1.0 %copy-done.1 = bf16[128,2048]{1,0:T(8,128)(2,1)S(1)} copy-done((bf16[128,2048]{1,0:T(8,128)(2,1)S(1)}, bf16[128,2048]{1,0:T(8,128)(2,1)}, u32[]{:S(2)}) %copy-start.1) | copy-done | bytes 524312
  4.2 0.0 copy-start.2
  4.2 1.0 %copy-done.2 = bf16[1,2048,128]{2,1,0:T(8,128)(2,1)S(1)} copy-done((bf16[1,2048,128]{2,1,0:T(8,128)(2,1)S(1)}, bf16[1,2048,128]{2,1,0:T(8,128)(2,1)}, u32[]{:S(2)}) %copy-start.2) | copy-done | bytes 524312
  5.2 0.0 copy-start.3
  5.2 1.0 %copy-done.3 = bf16[1,2048,128]{2,1,0:T(8,128)(2,1)S(1)} copy-done((bf16[1,2048,128]{2,1,0:T(8,128)(2,1)S(1)}, bf16[1,2048,128]{2,1,0:T(8,128)(2,1)}, u32[]{:S(2)}) %copy-start.3) | copy-done | bytes 524312
  6.3 0.0 copy-start.4
  6.3 1.0 %copy-done.4 = bf16[1,128,2048]{2,1,0:T(8,128)(2,1)S(1)} copy-done((bf16[1,128,2048]{2,1,0:T(8,128)(2,1)S(1)}, bf16[1,128,2048]{2,1,0:T(8,128)(2,1)}, u32[]{:S(2)}) %copy-start.4) | copy-done | bytes 524312
  7.3 43.2 %shard_map.134 = (bf16[128,256]{1,0:T(8,128)(2,1)S(1)}, f32[128,2]{1,0:T(8,128)S(1)}, f32[2048,128]{1,0:T(8,128)S(1)}, f32[2048,128]{1,0:T(8,128)S(1)}, f32[128,...) custom-call(bf16[128,2048]{1,0:T(8,128)(2,1)S(1)} %copy-done, ...), custom_call_target="tpu_custom_call" | custom-call | tf_op jit(solution)/shard_map/pallas_call | solution.py:321
  50.5 0.6 %copy.17 = f32[128,2]{0,1:T(2,128)} copy(f32[128,2]{1,0:T(8,128)S(1)} %get-tuple-element.25) | data formatting | bytes 2048
  51.1 0.6 %copy.25 = bf16[128,256]{1,0:T(8,128)(2,1)} copy(bf16[128,256]{1,0:T(8,128)(2,1)S(1)} %get-tuple-element.40) | data formatting | bytes 131072
  51.8 1.0 %copy.26 = f32[1,2048,128]{2,1,0:T(8,128)} copy(f32[1,2048,128]{2,1,0:T(8,128)S(1)} %bitcast.8) | data formatting | bytes 2097152
  52.7 1.0 %copy.27 = f32[1,2048,128]{2,1,0:T(8,128)} copy(f32[1,2048,128]{2,1,0:T(8,128)S(1)} %bitcast.7) | data formatting | bytes 2097152
  53.7 1.0 %copy.28 = f32[1,128,2048]{2,1,0:T(8,128)} copy(f32[1,128,2048]{2,1,0:T(8,128)S(1)} %bitcast.6) | data formatting | bytes 2097152
  54.7 0.6 %copy.29 = f32[1,2048]{1,0:T(1,128)} copy(f32[1,2048]{1,0:T(1,128)S(1)} %get-tuple-element.45) | data formatting | bytes 16384
  55.3 0.6 %copy.30 = f32[1,2048]{1,0:T(1,128)} copy(f32[1,2048]{1,0:T(1,128)S(1)} %get-tuple-element.46) | data formatting | bytes 16384
  55.9 0.5 copy.31
Async XLA Ops:
  0.6 0.7 %copy-start.5 = (s32[128,2]{0,1:T(2,128)S(1)}, s32[128,2]{0,1:T(2,128)}, u32[]{:S(2)}) copy-start(s32[128,2]{0,1:T(2,128)} %param.8) | copy-start | bytes 3076
  1.3 0.7 %copy-start.6 = (f32[128,2]{0,1:T(2,128)S(1)}, f32[128,2]{0,1:T(2,128)}, u32[]{:S(2)}) copy-start(f32[128,2]{0,1:T(2,128)} %param.9) | copy-start | bytes 3076
  2.1 1.0 %copy-start = (bf16[128,2048]{1,0:T(8,128)(2,1)S(1)}, bf16[128,2048]{1,0:T(8,128)(2,1)}, u32[]{:S(2)}) copy-start(bf16[128,2048]{1,0:T(8,128)(2,1)} %tok_ref.1) | copy-start | bytes 1572868
  3.1 1.0 %copy-start.1 = (bf16[128,2048]{1,0:T(8,128)(2,1)S(1)}, bf16[128,2048]{1,0:T(8,128)(2,1)}, u32[]{:S(2)}) copy-start(bf16[128,2048]{1,0:T(8,128)(2,1)} %cot_ref.1) | copy-start | bytes 1572868
  4.2 1.0 %copy-start.2 = (bf16[1,2048,128]{2,1,0:T(8,128)(2,1)S(1)}, bf16[1,2048,128]{2,1,0:T(8,128)(2,1)}, u32[]{:S(2)}) copy-start(bf16[1,2048,128]{2,1,0:T(8,128)(2,1)} %param.11) | copy-start | bytes 1572868
  5.2 1.0 %copy-start.3 = (bf16[1,2048,128]{2,1,0:T(8,128)(2,1)S(1)}, bf16[1,2048,128]{2,1,0:T(8,128)(2,1)}, u32[]{:S(2)}) copy-start(bf16[1,2048,128]{2,1,0:T(8,128)(2,1)} %param.12) | copy-start | bytes 1572868
  6.3 1.0 %copy-start.4 = (bf16[1,128,2048]{2,1,0:T(8,128)(2,1)S(1)}, bf16[1,128,2048]{2,1,0:T(8,128)(2,1)}, u32[]{:S(2)}) copy-start(bf16[1,128,2048]{2,1,0:T(8,128)(2,1)} %param.13) | copy-start | bytes 1572868

commit v2 on v1

--- a/solution.py
+++ b/solution.py
@@ -39,13 +39,14 @@
 
 def kernel(
     ep, tp, cap,
+    tok_hbm, routes_hbm, gates_hbm, cot_hbm, wg_hbm, wl_hbm, wd_hbm,
+    dtok_ref, dgate_ref, gw_v, lw_v, dw_v, gn_ref, ln_ref, dn_ref,
     tok_ref, routes_ref, gates_ref, cot_ref, wg_ref, wl_ref, wd_ref,
-    dtok_ref, dgate_ref, gw_ref, lw_ref, dw_ref, gn_ref, ln_ref, dn_ref,
-    pt_v, snd_v, all_v, gsnd_v, grow_v, bf_v, tr_v,
+    pt_v, pk_v, snd_v, all_v, gsnd_v, grow_v, bf_v, tr_v,
     ps_v, pr_v, mine_v, xs_v, ret_v, zs_v, zr_v,
-    gp_v, gsum_v, gback_v, ns_v, nr_v, gw_v, lw_v, dw_v,
-    d_s, d_r, g_s, g_r, y_s, y_r, p_s, p_r, x_s, x_r, z_s, z_r,
-    a_s, a_r, b_s, b_r, n_s, n_r, o_s,
+    gp_v, gsum_v, gback_v, ns_v, nr_v,
+    d_s, d_r, h_s, h_r, g_s, g_r, y_s, y_r, p_s, p_r, x_s, x_r, z_s, z_r,
+    a_s, a_r, b_s, b_r, n_s, n_r, l_s,
 ):
     me = lax.axis_index("ep")
     tpi = lax.axis_index("tp")
@@ -59,6 +60,16 @@
     hidden_units = wg_ref.shape[1]
     half = width // CORES
     own = width // tp
+    odd = lax.rem(chip, 2)
+    beside = (chip + 1 - 2 * odd) * CORES + core
+    loads = []
+    for i, (src, dst) in enumerate((
+        (routes_hbm, routes_ref), (gates_hbm, gates_ref), (cot_hbm, cot_ref),
+        (tok_hbm, tok_ref), (wg_hbm, wg_ref), (wl_hbm, wl_ref), (wd_hbm, wd_ref),
+    )):
+        cp = pltpu.make_async_copy(src, dst, l_s.at[i])
+        cp.start()
+        loads.append(cp)
 
     def ahead(r):
         return lax.rem(me + r, ep)
@@ -80,49 +91,95 @@
             device_id=where, device_id_type=MESH,
         )
 
+    loads[0].wait()
+    loads[1].wait()
     rel = routes_ref[...] - me
     rel = jnp.where(rel < 0, rel + ep, rel)
-    lane = lax.broadcasted_iota(jnp.int32, (rows, LANES), 1)
-    first, second = lane == rel[:, 0:1], lane == rel[:, 1:2]
+    erows = gp_v.shape[1]
+    sub = lax.broadcasted_iota(jnp.int32, (erows, rows), 0)
+    first, second = sub == rel[0:1, :], sub == rel[1:2, :]
     mask = jnp.where(first, 1.0, 0.0) + jnp.where(second, 1.0, 0.0)
-    gate_of = jnp.where(first, gates_ref[:, 0:1], 0.0) + jnp.where(second, gates_ref[:, 1:2], 0.0)
-    before = lax.broadcasted_iota(jnp.int32, (rows, rows), 1) < lax.broadcasted_iota(
-        jnp.int32, (rows, rows), 0
-    )
-    rank = dot_nn(jnp.where(before, 1.0, 0.0).astype(bf16), mask.astype(bf16))
+    gate_of = jnp.where(first, gates_ref[0:1, :], 0.0) + jnp.where(second, gates_ref[1:2, :], 0.0)
+    before = lax.broadcasted_iota(jnp.int32, (rows, rows), 0) < lax.broadcasted_iota(
+        jnp.int32, (rows, rows), 1
+    )
+    rank = dot_nn(mask.astype(bf16), jnp.where(before, 1.0, 0.0).astype(bf16))
     place = jnp.where(mask > 0.5, rank, -1.0)
-    lane_f = lane.astype(f32)
+    slot_at = lax.broadcasted_iota(jnp.int32, (LANES, rows), 0).astype(f32)
+    hits = [jnp.where(slot_at == place[r:r + 1, :], 1.0, 0.0) for r in range(ep)]
+    picks = [hit[:cap, :].astype(bf16) for hit in hits]
+    square = lax.broadcasted_iota(jnp.int32, (LANES, LANES), 0) == lax.broadcasted_iota(
+        jnp.int32, (LANES, LANES), 1
+    )
     sends = []
-    picks = []
+
+    narrow = half // 8
+    pieces = (
+        (1, 0, half // 2, True),
+        (0, 0, narrow, True),
+        (0, 2 * narrow, half - 2 * narrow, False),
+    )
+    swapped = [i for i, piece in enumerate(pieces) if piece[3]]
+    refs = (tok_ref, cot_ref)
+
+    def window(i, whose):
+        a, off, w, shared = pieces[i]
+        if shared:
+            off = off + whose * w
+        return a, (pl.ds(pl.multiple_of(off, LANES), w) if shared else pl.ds(off, w))
+
+    def area(buf, i, r, whose, which):
+        a, cols = window(i, whose)
+        return buf.at[a, which, pl.ds(r * cap, cap), cols]
+
+    def dispatch(i, r):
+        a, cols = window(i, odd)
+        return remote(
+            snd_v.at[a, r, :, cols], area(all_v, i, r, odd, core),
+            d_s.at[i, r], d_r.at[i, r], {"ep": ahead(r)},
+        )
+
+    def swap(i, r, whose):
+        at = area(all_v, i, r, whose, core)
+        return remote(at, at, h_s.at[i, r], h_r.at[i, r], {"tp": beside})
+
+    def relay(k, i, r, whose, which):
+        at = area(all_v, i, r, whose, which)
+        return remote(at, at, y_s.at[k, r], y_r.at[k, r], {"tp": partner})
+
+    loads[2].wait()
+    loads[3].wait()
+    waited = False
+    for i in range(len(pieces)):
+        a, off, w, shared = pieces[i]
+        start = core * half + off + (odd * w if shared else 0)
+        src_cols = pl.ds(pl.multiple_of(start, LANES), w)
+        for r in range(1, ep):
+            snd_v[a, r, :, window(i, odd)[1]] = dot_nn(
+                picks[r], refs[a][:, src_cols]
+            ).astype(bf16)
+            if not waited:
+                pl.semaphore_wait(barrier, ep - 1 + tp - 1)
+                waited = True
+            cp = dispatch(i, r)
+            cp.start()
+            sends.append(cp)
     for r in range(ep):
-        hit = jnp.where(lane_f == place[:, r:r + 1], 1.0, 0.0)
-        pt_v[r] = hit.astype(bf16)
-        picks.append(hit.T[:cap, :].astype(bf16))
-        row = jnp.sum(hit * gate_of[:, r:r + 1], axis=0, keepdims=True)
+        col = jnp.sum(hits[r] * gate_of[r:r + 1, :], axis=1, keepdims=True)
+        row = jnp.sum(jnp.where(square, col, 0.0), axis=0, keepdims=True)
         if r == 0:
             grow_v[0] = jnp.broadcast_to(row, (8, LANES))
         else:
             gsnd_v[r] = jnp.broadcast_to(row, (8, LANES))
-    half_cols = pl.ds(pl.multiple_of(core * half, half), half)
-    waited = False
-    for r in range(1, ep):
-        for a, ref in ((0, tok_ref), (1, cot_ref)):
-            snd_v[a, r] = dot_nn(picks[r], ref[:, half_cols]).astype(bf16)
-            if not waited:
-                pl.semaphore_wait(barrier, ep - 1 + tp - 1)
-                waited = True
-            cp = remote(
-                snd_v.at[a, r], all_v.at[a, core, pl.ds(r * cap, cap), :],
-                d_s.at[a, r], d_r.at[a, r], {"ep": ahead(r)},
-            )
+            cp = remote(gsnd_v.at[r], grow_v.at[r], g_s.at[r], g_r.at[r], {"ep": ahead(r)})
             cp.start()
             sends.append(cp)
-        cp = remote(gsnd_v.at[r], grow_v.at[r], g_s.at[r], g_r.at[r], {"ep": ahead(r)})
-        cp.start()
-        sends.append(cp)
     for a, ref in ((0, tok_ref), (1, cot_ref)):
         for h in range(CORES):
             all_v[a, h, 0:cap, :] = dot_nn(picks[0], ref[:, h * half:(h + 1) * half]).astype(bf16)
+    for r in range(ep):
+        pk_v[r] = hits[r].astype(bf16)
+        pt_v[r] = hits[r].T.astype(bf16)
 
     eye = lax.broadcasted_iota(jnp.int32, (cap, LANES), 0) == lax.broadcasted_iota(
         jnp.int32, (cap, LANES), 1
@@ -148,19 +205,33 @@
         bf_v[1, rs, :] = lin_bf
         bf_v[2, rs, :] = (gate_col * hidden).astype(bf16)
 
+    count = len(pieces)
+    for i in swapped:
+        for r in range(1, ep):
+            dispatch(i, r).wait_recv()
+            for cp in (swap(i, r, odd), relay(i, i, r, odd, core)):
+                cp.start()
+                sends.append(cp)
+    for cp in loads[4:]:
+        cp.wait()
     forward(0)
-    relays = []
     for r in range(1, ep):
-        for a in range(2):
-            mine = all_v.at[a, core, pl.ds(r * cap, cap), :]
-            remote(snd_v.at[a, r], mine, d_s.at[a, r], d_r.at[a, r], {"ep": ahead(r)}).wait_recv()
-            cp = remote(mine, mine, y_s.at[a, r], y_r.at[a, r], {"tp": partner})
+        for n, i in enumerate(swapped):
+            swap(i, r, 1 - odd).wait_recv()
+            cp = relay(count + n, i, r, 1 - odd, core)
             cp.start()
-            relays.append(cp)
+            sends.append(cp)
+        for i in range(count):
+            if i not in swapped:
+                dispatch(i, r).wait_recv()
+                cp = relay(i, i, r, odd, core)
+                cp.start()
+                sends.append(cp)
     for r in range(1, ep):
-        for a in range(2):
-            theirs = all_v.at[a, other, pl.ds(r * cap, cap), :]
-            remote(theirs, theirs, y_s.at[a, r], y_r.at[a, r], {"tp": partner}).wait_recv()
+        for i in range(count):
+            relay(i, i, r, odd, other).wait_recv()
+        for n, i in enumerate(swapped):
+            relay(count + n, i, r, 1 - odd, other).wait_recv()
         remote(gsnd_v.at[r], grow_v.at[r], g_s.at[r], g_r.at[r], {"ep": ahead(r)}).wait_recv()
         forward(r)
 
@@ -201,7 +272,6 @@
     for i in range(3):
         tr_v[i] = bf_v[i].astype(f32).T.astype(bf16)
     step = min(512, half)
-    outs = []
     for h in range(CORES):
         for c0 in range(0, half, step):
             cols = slice(h * half + c0, h * half + c0 + step)
@@ -215,10 +285,6 @@
         cp = remote(ns_v, nr_v.at[tpi], n_s.at[q], n_r.at[q], {"tp": lax.rem(tpi + q, tp)})
         cp.start()
         sends.append(cp)
-    for i, (src, dst) in enumerate(((gw_v, gw_ref), (lw_v, lw_ref))):
-        cp = pltpu.make_async_copy(src, dst, o_s.at[i])
-        cp.start()
-        outs.append(cp)
 
     for q in range(1, tp):
         frm = lax.rem(tpi + tp - q, tp)
@@ -240,9 +306,6 @@
             w = dot_nn(tr_v[2], all_v[1, h, :, c0:c0 + step])
             norm = norm + jnp.sum(w * w, axis=1, keepdims=True)
             dw_v[:, cols] = w
-    cp = pltpu.make_async_copy(dw_v, dw_ref, o_s.at[2])
-    cp.start()
-    outs.append(cp)
     diag = lax.broadcasted_iota(jnp.int32, (hidden_units, hidden_units), 0) == (
         lax.broadcasted_iota(jnp.int32, (hidden_units, hidden_units), 1)
     )
@@ -269,17 +332,18 @@
             cp.start()
             sends.append(cp)
 
-    res = [jnp.zeros((rows, 1), f32), jnp.zeros((rows, 1), f32)]
+    res = [jnp.zeros((1, rows), f32), jnp.zeros((1, rows), f32)]
     for r in range(ep):
         if r > 0:
             remote(
                 gsum_v.at[r], gback_v.at[r], b_s.at[r], b_r.at[r], {"ep": behind(r)}
             ).wait_recv()
-        val = jnp.sum(pt_v[r].astype(f32) * gback_v[r, 0:1, :], axis=1, keepdims=True)
+        col = jnp.sum(jnp.where(square, gback_v[r, 0:1, :], 0.0), axis=1, keepdims=True)
+        val = jnp.sum(pk_v[r].astype(f32) * col, axis=0, keepdims=True)
         for k in range(2):
-            res[k] = res[k] + jnp.where(rel[:, k:k + 1] == r, val, 0.0)
-    dgate_ref[:, 0:1] = res[0]
-    dgate_ref[:, 1:2] = res[1]
+            res[k] = res[k] + jnp.where(rel[k:k + 1, :] == r, val, 0.0)
+    dgate_ref[0:1, :] = res[0]
+    dgate_ref[1:2, :] = res[1]
 
     for q in range(1, tp):
         frm = lax.rem(tpi + tp - q, tp)
@@ -295,9 +359,18 @@
         acc = acc + zr_v[q].astype(f32)
     dtok_ref[...] = acc.astype(bf16)
 
-    for cp in sends + relays:
+    for cp in sends:
         cp.wait_send()
-    for cp in outs:
+
+
+def write_out(*refs):
+    count = (len(refs) - 1) // 2
+    copies = [
+        pltpu.make_async_copy(refs[i], refs[count + i], refs[-1].at[i]) for i in range(count)
+    ]
+    for cp in copies:
+        cp.start()
+    for cp in copies:
         cp.wait()
 
 
@@ -314,25 +387,34 @@
     own = width // tp
     nz = tp // CORES
     vm = pl.BlockSpec(memory_space=pltpu.VMEM)
-    hbm = pl.BlockSpec(memory_space=pl.ANY)
+    hbm = pl.BlockSpec(memory_space=pltpu.HBM)
     dma = pltpu.SemaphoreType.DMA
     erows = max(8, ep)
     V = pltpu.VMEM
+    out_shape = (
+        jax.ShapeDtypeStruct((rows, own), bf16),
+        jax.ShapeDtypeStruct((top, rows), f32),
+        jax.ShapeDtypeStruct((width, units), f32),
+        jax.ShapeDtypeStruct((width, units), f32),
+        jax.ShapeDtypeStruct((units, width), f32),
+        jax.ShapeDtypeStruct((1, width), f32),
+        jax.ShapeDtypeStruct((1, width), f32),
+        jax.ShapeDtypeStruct((1, units), f32),
+    )
     outs = pl.pallas_call(
         functools.partial(kernel, ep, tp, cap),
-        out_shape=(
-            jax.ShapeDtypeStruct((rows, own), bf16),
-            jax.ShapeDtypeStruct((rows, top), f32),
-            jax.ShapeDtypeStruct((width, units), f32),
-            jax.ShapeDtypeStruct((width, units), f32),
-            jax.ShapeDtypeStruct((units, width), f32),
-            jax.ShapeDtypeStruct((1, width), f32),
-            jax.ShapeDtypeStruct((1, width), f32),
-            jax.ShapeDtypeStruct((1, units), f32),
-        ),
-        in_specs=[vm] * 7,
-        out_specs=(vm, vm, hbm, hbm, hbm, vm, vm, vm),
+        out_shape=out_shape,
+        in_specs=[hbm] * 7,
+        out_specs=(vm,) * 8,
         scratch_shapes=[
+            V((rows, width), bf16),
+            V((top, rows), jnp.int32),
+            V((top, rows), f32),
+            V((rows, width), bf16),
+            V((width, units), bf16),
+            V((width, units), bf16),
+            V((units, width), bf16),
+            V((ep, rows, LANES), bf16),
             V((ep, rows, LANES), bf16),
             V((2, ep, cap, half), bf16),
             V((2, CORES, slots, half), bf16),
@@ -352,19 +434,27 @@
             V((ep, 8, LANES), f32),
             V((2, width), f32),
             V((tp, 2, width), f32),
-            V((width, units), f32),
-            V((width, units), f32),
-            V((units, width), f32),
-            dma((2, ep)), dma((2, ep)), dma((ep,)), dma((ep,)), dma((2, ep)), dma((2, ep)),
+            dma((3, ep)), dma((3, ep)), dma((2, ep)), dma((2, ep)), dma((ep,)), dma((ep,)),
+            dma((5, ep)), dma((5, ep)),
             dma((nz,)), dma((nz,)), dma((nz, ep)), dma((nz, ep)), dma((nz,)), dma((nz,)),
-            dma((tp,)), dma((tp,)), dma((ep,)), dma((ep,)), dma((tp,)), dma((tp,)), dma((3,)),
+            dma((tp,)), dma((tp,)), dma((ep,)), dma((ep,)), dma((tp,)), dma((tp,)), dma((7,)),
         ],
         compiler_params=pltpu.CompilerParams(
-            collective_id=0, has_side_effects=True, vmem_limit_bytes=40 * 1024 * 1024
+            collective_id=0, has_side_effects=True, vmem_limit_bytes=28 * 1024 * 1024
         ),
-    )(tokens, routes, gates, cotangent, w_glu[0], w_lin[0], w_down[0])
+    )(*(pltpu.with_memory_space_constraint(x, pltpu.HBM) for x in (
+        tokens, routes.T, gates.T, cotangent, w_glu[0], w_lin[0], w_down[0]
+    )))
+    outs = pl.pallas_call(
+        write_out,
+        out_shape=out_shape,
+        in_specs=[vm] * len(out_shape),
+        out_specs=(hbm,) * len(out_shape),
+        scratch_shapes=[dma((len(out_shape),))],
+        compiler_params=pltpu.CompilerParams(vmem_limit_bytes=28 * 1024 * 1024),
+    )(*outs)
     d_tokens, d_gates, gw, lw, dw, gn, ln, dn = outs
-    return (d_tokens, d_gates, gw[None], lw[None], dw[None], gn, ln, dn)
+    return (d_tokens, d_gates.T, gw[None], lw[None], dw[None], gn, ln, dn)
 
 
 def solution(mesh):

time: 56.8 us -> 41.6 us (0.73)
  local copies, waits for them, and re-layouts: 12.5 us -> 0 us
  Pallas kernels: 43.2 us -> 40.8 us
    unnamed x24 -> x0, local copies, waits for them, and re-layouts: 12.5 us -> none
    pallas_call x1 -> x2, Pallas kernels: 43.2 us -> 40.8 us  [the longest x1 39 us: shards(): pl.pallas_call(functools.partial(kernel, ep, tp, cap), out_shape=out_shap...]
where the time goes in v2:
time: 41.6 us; the launch traced here: 41.4 us
  Pallas kernels  40.8 us (98%)
  between operations  0.64 us (2%)
    pallas_call x1, Pallas kernels, shards(): pl.pallas_call(functools.partial(kernel, ep, tp, cap), out_shape=out_shap...  39 us
    pallas_call x1, Pallas kernels, shards(): pl.pallas_call(write_out, out_shape=out_shape, in_specs=[vm] * len(out_sh...  1.77 us

profile of v2, /device:TPU:0, one launch (start us, length us, event | category | flops | bytes accessed | tf_op | source)
XLA Modules:
  0.0 41.4 jit_solution(9500275171075646377)
XLA Ops:
  0.6 39.0 %shard_map.134 = (bf16[128,256]{1,0:T(8,128)(2,1)S(1)}, f32[2,128]{1,0:T(2,128)S(1)}, f32[2048,128]{1,0:T(8,128)S(1)}, f32[2048,128]{1,0:T(8,128)S(1)}, f32[128,...) custom-call(bf16[128,2048]{1,0:T(8,128)(2,1)} %tok_hbm.1, ...), custom_call_target="tpu_custom_call" | custom-call | tf_op jit(solution)/shard_map/pallas_call | solution.py:404
  39.7 1.8 %shard_map.135 = (bf16[128,256]{1,0:T(8,128)(2,1)}, f32[2,128]{1,0:T(2,128)}, f32[2048,128]{1,0:T(8,128)}, f32[2048,128]{1,0:T(8,128)}, f32[128,2048]{1,0:T(8,12...) custom-call(bf16[128,256]{1,0:T(8,128)(2,1)S(1)} %get-tuple-element.24.refs_0_, ...), custom_call_target="tpu_custom_call" | custom-call | tf_op jit(solution)/shard_map/pallas_call | solution.py:448

commit v3 on v2

--- a/solution.py
+++ b/solution.py
@@ -214,8 +214,35 @@
                 sends.append(cp)
     for cp in loads[4:]:
         cp.wait()
-    forward(0)
-    for r in range(1, ep):
+    order = list(range(1, nz)) + [0]
+
+    def input_cols(q, which, rs):
+        z = lax.rem(chip + q, nz)
+        at = pl.ds(pl.multiple_of((z * CORES + which) * own, own), own)
+        return dot_nt(bf_v[0, rs, :], wg_ref[at, :]) + dot_nt(bf_v[1, rs, :], wl_ref[at, :])
+
+    def to_partner(r):
+        at = pl.ds(r * cap, cap)
+        return remote(ps_v.at[:, at, :], pr_v.at[:, at, :], p_s.at[r], p_r.at[r], {"tp": partner})
+
+    def block(r):
+        if r > 0:
+            for i in range(count):
+                relay(i, i, r, odd, other).wait_recv()
+            for n, i in enumerate(swapped):
+                relay(count + n, i, r, 1 - odd, other).wait_recv()
+            remote(gsnd_v.at[r], grow_v.at[r], g_s.at[r], g_r.at[r], {"ep": ahead(r)}).wait_recv()
+        forward(r)
+        rs = slice(r * cap, (r + 1) * cap)
+        for q in order:
+            ps_v[q, rs, :] = input_cols(q, other, rs).astype(bf16)
+        cp = to_partner(r)
+        cp.start()
+        sends.append(cp)
+        for q in order:
+            mine_v[q, rs, :] = input_cols(q, core, rs)
+
+    def arrive(r):
         for n, i in enumerate(swapped):
             swap(i, r, 1 - odd).wait_recv()
             cp = relay(count + n, i, r, 1 - odd, core)
@@ -227,34 +254,19 @@
                 cp = relay(i, i, r, odd, core)
                 cp.start()
                 sends.append(cp)
-    for r in range(1, ep):
-        for i in range(count):
-            relay(i, i, r, odd, other).wait_recv()
-        for n, i in enumerate(swapped):
-            relay(count + n, i, r, 1 - odd, other).wait_recv()
-        remote(gsnd_v.at[r], grow_v.at[r], g_s.at[r], g_r.at[r], {"ep": ahead(r)}).wait_recv()
-        forward(r)
-
-    for q in range(1, tp):
-        cp = remote(gp_v.at[tpi], gp_v.at[tpi], a_s.at[q], a_r.at[q], {"tp": lax.rem(tpi + q, tp)})
-        cp.start()
-        sends.append(cp)
-
-    def input_cols(q, which):
-        z = lax.rem(chip + q, nz)
-        at = pl.ds(pl.multiple_of((z * CORES + which) * own, own), own)
-        return dot_nt(bf_v[0], wg_ref[at, :]) + dot_nt(bf_v[1], wl_ref[at, :])
-
-    order = list(range(1, nz)) + [0]
+
+    middle = ep // 2
+    turn = [middle] + [r for r in range(1, ep) if r != middle]
+    block(0)
+    for n, r in enumerate(turn):
+        arrive(r)
+        if n > 0:
+            block(turn[n - 1])
+    block(turn[-1])
+
+    for r in range(ep):
+        to_partner(r).wait_recv()
     for q in order:
-        ps_v[q] = input_cols(q, other).astype(bf16)
-        cp = remote(ps_v.at[q], pr_v.at[q], p_s.at[q], p_r.at[q], {"tp": partner})
-        cp.start()
-        sends.append(cp)
-    for q in order:
-        mine_v[q] = input_cols(q, core)
-    for q in order:
-        remote(ps_v.at[q], pr_v.at[q], p_s.at[q], p_r.at[q], {"tp": partner}).wait_recv()
         total = (mine_v[q] + pr_v[q].astype(f32)).astype(bf16)
         ret_v[q, 0:cap, :] = total[0:cap, :]
         for r in range(1, ep):
@@ -268,6 +280,11 @@
             )
             cp.start()
             sends.append(cp)
+
+    for q in range(1, tp):
+        cp = remote(gp_v.at[tpi], gp_v.at[tpi], a_s.at[q], a_r.at[q], {"tp": lax.rem(tpi + q, tp)})
+        cp.start()
+        sends.append(cp)
 
     for i in range(3):
         tr_v[i] = bf_v[i].astype(f32).T.astype(bf16)
@@ -436,7 +453,7 @@
             V((tp, 2, width), f32),
             dma((3, ep)), dma((3, ep)), dma((2, ep)), dma((2, ep)), dma((ep,)), dma((ep,)),
             dma((5, ep)), dma((5, ep)),
-            dma((nz,)), dma((nz,)), dma((nz, ep)), dma((nz, ep)), dma((nz,)), dma((nz,)),
+            dma((ep,)), dma((ep,)), dma((nz, ep)), dma((nz, ep)), dma((nz,)), dma((nz,)),
             dma((tp,)), dma((tp,)), dma((ep,)), dma((ep,)), dma((tp,)), dma((tp,)), dma((7,)),
         ],
         compiler_params=pltpu.CompilerParams(

time: 41.6 us -> 42.6 us (1.024)
  Pallas kernels: 40.8 us -> 41.8 us
    pallas_call x1, Pallas kernels: 39 us -> 40.1 us  [shards(): pl.pallas_call(functools.partial(kernel, ep, tp, cap), out_shape=out_shap...]
where the time goes in v3:
time: 42.6 us; the launch traced here: 42.5 us
  Pallas kernels  41.8 us (98%)
  between operations  0.64 us (2%)
    pallas_call x1, Pallas kernels, shards(): pl.pallas_call(functools.partial(kernel, ep, tp, cap), out_shape=out_shap...  40.1 us
    pallas_call x1, Pallas kernels, shards(): pl.pallas_call(write_out, out_shape=out_shape, in_specs=[vm] * len(out_sh...  1.77 us

profile of v3, /device:TPU:0, one launch (start us, length us, event | category | flops | bytes accessed | tf_op | source)
XLA Modules:
  0.0 42.5 jit_solution(17055789407891635111)
XLA Ops:
  0.6 40.1 %shard_map.134 = (bf16[128,256]{1,0:T(8,128)(2,1)S(1)}, f32[2,128]{1,0:T(2,128)S(1)}, f32[2048,128]{1,0:T(8,128)S(1)}, f32[2048,128]{1,0:T(8,128)S(1)}, f32[128,...) custom-call(bf16[128,2048]{1,0:T(8,128)(2,1)} %tok_hbm.1, ...), custom_call_target="tpu_custom_call" | custom-call | tf_op jit(solution)/shard_map/pallas_call | solution.py:421
  40.7 1.8 %shard_map.135 = (bf16[128,256]{1,0:T(8,128)(2,1)}, f32[2,128]{1,0:T(2,128)}, f32[2048,128]{1,0:T(8,128)}, f32[2048,128]{1,0:T(8,128)}, f32[128,2048]{1,0:T(8,12...) custom-call(bf16[128,256]{1,0:T(8,128)(2,1)S(1)} %get-tuple-element.24.refs_0_, ...), custom_call_target="tpu_custom_call" | custom-call | tf_op jit(solution)/shard_map/pallas_call | solution.py:465
